TPU v7x, 32 devices: a whole 2x2x4 slice. The times are simulated.
32 devices in a mesh: fs: 4 (over z), tp: 8 (over y, x, core).
Axes of the slice: x: 2, y: 2, z: 4, core: 2. Of those that a mesh axis runs over, the one named last changes fastest.
Arguments:
- block_in: bfloat16 [4096, 2304], P('fs'), may hold values from -6 to 6
- out_cot: bfloat16 [4096, 2304], P('fs'), may hold values from -6 to 6
- gated_out: bfloat16 [4096, 4608], P('fs', 'tp'), may hold values from -6 to 6
- gate_cot: bfloat16 [4096, 4608], P('fs', 'tp'), may hold values from -6 to 6
- factor_out: bfloat16 [2304, 192], P('fs'), may hold values from -0.104166667 to 0.104166667
- factor_z: bfloat16 [2304, 192], P('fs'), may hold values from -0.104166667 to 0.104166667
- weight_out: float32 [4608, 2304], P('tp', 'fs'), may hold values from -0.09375 to 0.09375
- weight_z: float32 [2304, 4608], P('fs', 'tp'), may hold values from -0.125 to 0.125
- first_out: float32 [4608, 192], P('tp', 'fs'), may hold values from -512 to 512
- second_out: float32 [4608, 192], P('tp', 'fs'), may hold values from 819.2 to 20480
- first_z: float32 [192, 4608], P('fs', 'tp'), may hold values from -512 to 512
- second_z: float32 [192, 4608], P('fs', 'tp'), may hold values from 819.2 to 20480
Outputs:
- step_out: float32 [4608, 2304], P('tp', 'fs')
- step_z: float32 [2304, 4608], P('fs', 'tp')
- new_first_out: float32 [4608, 192], P('tp', 'fs')
- new_second_out: float32 [4608, 192], P('tp', 'fs')
- new_first_z: float32 [192, 4608], P('fs', 'tp')
- new_second_z: float32 [192, 4608], P('fs', 'tp')
- copy_out: bfloat16 [4608, 2304], P('tp')
- copy_z: bfloat16 [2304, 4608], P(None, 'tp')
All inputs are finite; a program needn't handle non-finite values.
Results may differ from a plain program's by a relative error of at most 0.0018.
Values may be sent and summed in bfloat16 or wider, within the bound.
A program may use at most 64 MiB of HBM per device.

v0:
```python
import jax
import jax.numpy as jnp
from jax import lax
from jax.sharding import PartitionSpec as P

D = 2304
INNER = 4608


beta_first = 0.8
beta_second = 0.9
adam_eps = 1e-08
norm_eps = 1e-06
rate = 0.005


def moments(first, second, gradient):
    new_first = beta_first * first + (1.0 - beta_first) * gradient
    new_second = beta_second * second + (1.0 - beta_second) * gradient * gradient
    return (new_first, new_second, new_first / (jnp.sqrt(new_second) + adam_eps))


def split_parts(values):
    high_part = values.astype(jnp.bfloat16)
    low_part = (values - high_part.astype(jnp.float32)).astype(jnp.bfloat16)
    return (high_part, low_part)


def per_device(
    block_in,
    out_cot,
    gated_out,
    gate_cot,
    factor_out,
    factor_z,
    weight_out,
    weight_z,
    first_out,
    second_out,
    first_z,
    second_z,
):
    sum_cot = jnp.dot(
        out_cot,
        lax.all_gather(factor_out, "fs", axis=0, tiled=True),
        preferred_element_type=jnp.float32,
    )
    sum_input = jnp.dot(
        block_in,
        lax.all_gather(factor_z, "fs", axis=0, tiled=True),
        preferred_element_type=jnp.float32,
    )
    cot_high, cot_low = split_parts(sum_cot)
    input_high, input_low = split_parts(sum_input)
    term_out = jnp.dot(gated_out.T, cot_high, preferred_element_type=jnp.float32) + jnp.dot(
        gated_out.T, cot_low, preferred_element_type=jnp.float32
    )
    term_z = jnp.dot(input_high.T, gate_cot, preferred_element_type=jnp.float32) + jnp.dot(
        input_low.T, gate_cot, preferred_element_type=jnp.float32
    )
    grad_out, grad_z = (
        lax.psum_scatter(term_out, "fs", scatter_dimension=1, tiled=True),
        lax.psum_scatter(term_z, "fs", scatter_dimension=0, tiled=True),
    )
    new_first_out, new_second_out, part_out = moments(first_out, second_out, grad_out)
    new_first_z, new_second_z, part_z = moments(first_z, second_z, grad_z)
    dir_out, dir_z = (
        lax.all_gather(part_out, "fs", axis=1, tiled=True),
        lax.all_gather(part_z, "fs", axis=0, tiled=True),
    )
    update_out = jnp.dot(dir_out, factor_out.astype(jnp.float32).T, precision=lax.Precision.HIGHEST)
    update_z = jnp.dot(factor_z.astype(jnp.float32), dir_z, precision=lax.Precision.HIGHEST)
    total_out, total_z = lax.psum(
        (jnp.sum(update_out * update_out), jnp.sum(update_z * update_z)), ("fs", "tp")
    )
    entries = D * INNER
    step_out = update_out * lax.rsqrt(total_out / entries + norm_eps)
    step_z = update_z * lax.rsqrt(total_z / entries + norm_eps)
    fresh_out = (weight_out - rate * step_out).astype(jnp.bfloat16)
    fresh_z = (weight_z - rate * step_z).astype(jnp.bfloat16)
    copy_out, copy_z = (
        lax.all_gather(fresh_out, "fs", axis=1, tiled=True),
        lax.all_gather(fresh_z, "fs", axis=0, tiled=True),
    )
    return (
        step_out,
        step_z,
        new_first_out,
        new_second_out,
        new_first_z,
        new_second_z,
        copy_out,
        copy_z,
    )


def solution(mesh):
    return jax.shard_map(
        per_device,
        mesh=mesh,
        in_specs=(
            P("fs", None),
            P("fs", None),
            P("fs", "tp"),
            P("fs", "tp"),
            P("fs", None),
            P("fs", None),
            P("tp", "fs"),
            P("fs", "tp"),
            P("tp", "fs"),
            P("tp", "fs"),
            P("fs", "tp"),
            P("fs", "tp"),
        ),
        out_specs=(
            P("tp", "fs"),
            P("fs", "tp"),
            P("tp", "fs"),
            P("tp", "fs"),
            P("fs", "tp"),
            P("fs", "tp"),
            P("tp", None),
            P(None, "tp"),
        ),
        check_vma=False,
    )
```

profile of v0, /device:TPU:0, one launch (start us, length us, event | category | flops | bytes accessed | tf_op | source)
XLA Modules:
  0.0 295.9 jit_solution(130620478355484062)
XLA Ops:
  7.2 0.0 copy-start
  7.2 0.0 reduce-scatter.5.cloned.1.call-start
  7.2 23.8 %all-gather.1 = bf16[4,576,192]{1,2,0:T(8,128)(2,1)S(1)} all-gather(bf16[1,576,192]{1,2,0:T(8,128)(2,1)} %bitcast.24), channel_id=1, replica_groups=mesh['fs'=4,'tp'=8] {'fs'}, dimensions={0}, use_global_device_ids=true | all-gather | bytes 1105920 | tf_op jit(solution)/shard_map/all_gather | solution.py:50
  31.1 0.8 copy.27
  31.8 0.7 reshape.19
  32.5 4.0 %fusion.12 = f32[1024,192]{0,1:T(8,128)S(1)} fusion(bf16[1024,2304]{1,0:T(8,128)(2,1)} %param.12, bf16[2304,192]{0,1:T(8,128)(2,1)S(1)} %reshape.19), kind=kOutput, calls=%fused_computation.26 | convolution fusion | flops 905969664 | bytes 6389760 | tf_op jit(solution)/shard_map/dot_general | solution.py:48
  36.5 0.0 copy-done
  36.6 0.6 fusion.2
  37.2 0.0 copy-start.2
  37.2 1.4 convolution_add_fusion
  38.6 0.0 reduce-scatter.5.cloned.1.call-update
  38.6 0.0 reduce-scatter.3.cloned.1.call-start
  38.7 0.0 copy-done.2
  38.7 28.6 %all-gather = bf16[4,576,192]{1,2,0:T(8,128)(2,1)S(1)} all-gather(bf16[1,576,192]{1,2,0:T(8,128)(2,1)S(1)} %bitcast.23), channel_id=1, replica_groups=mesh['fs'=4,'tp'=8] {'fs'}, dimensions={0}, use_global_device_ids=true | all-gather | bytes 1105920 | tf_op jit(solution)/shard_map/all_gather | solution.py:45
  67.2 0.8 copy.26
  68.0 0.7 reshape.17
  68.7 0.0 copy-start.1
  68.7 4.1 %fusion.11 = f32[1024,192]{0,1:T(8,128)S(1)} fusion(bf16[1024,2304]{1,0:T(8,128)(2,1)} %param.13, bf16[2304,192]{0,1:T(8,128)(2,1)S(1)} %reshape.17), kind=kOutput, calls=%fused_computation.25 | convolution fusion | flops 905969664 | bytes 6389760 | tf_op jit(solution)/shard_map/dot_general | solution.py:43
  72.8 0.0 copy-done.1
  72.8 0.6 fusion.5
  73.4 0.0 copy-start.4
  73.4 0.0 copy-start.5
  73.5 1.4 fusion
  74.8 0.0 copy-start.6
  74.8 0.0 copy-start.7
  74.8 0.0 reduce-scatter.3.cloned.1.call-update
  74.9 0.0 all-gather.5.cloned.1.call-start
  74.9 0.0 reduce-scatter.5.cloned.1.call-done
  74.9 0.0 copy-done.4
  75.0 0.0 copy-done.5
  75.0 1.7 add_divide_fusion
  76.6 17.9 %all_gather.21 = f32[192,576]{1,0:T(8,128)S(1)} all-gather(f32[48,576]{1,0:T(8,128)S(1)} %get-tuple-element.38), channel_id=1, replica_groups=mesh['fs'=4,'tp'=8] {'fs'}, dimensions={0}, use_global_device_ids=true | all-gather | bytes 552960 | tf_op jit(solution)/shard_map/all_gather | solution.py:69
  94.5 3.4 %reduce-scatter.3.cloned.1.call-done = f32[576,48]{0,1:T(8,128)} async-done(((f32[576,192]{0,1:T(8,128)}), f32[576,48]{0,1:T(8,128)}) %reduce-scatter.3.cloned.1.call-update) | async-done | bytes 110608 | tf_op jit(solution)/shard_map/reduce_scatter | solution.py:62
  97.9 0.0 copy-done.6
  97.9 0.0 copy-done.7
  97.9 1.7 add_divide_fusion.1
  99.6 0.0 copy-start.3
  99.6 16.1 %all_gather.19 = f32[576,192]{0,1:T(8,128)S(1)} all-gather(f32[576,48]{0,1:T(8,128)S(1)} %get-tuple-element.41), channel_id=1, replica_groups=mesh['fs'=4,'tp'=8] {'fs'}, dimensions={1}, use_global_device_ids=true | all-gather | bytes 552960 | tf_op jit(solution)/shard_map/all_gather | solution.py:68
  115.6 2.8 multiply_reduce_fusion.1
  118.4 0.0 copy-done.3
  118.4 1.6 multiply_reduce_fusion
  120.0 38.5 %all-reduce = (f32[]{:T(128)}, f32[]{:T(128)}) all-reduce(f32[]{:T(128)} %get-tuple-element.44, f32[]{:T(128)} %get-tuple-element.46), channel_id=1, replica_groups=mesh['fs'=4,'tp'=8] {'fs','tp'}, use_global_device_ids=true, to_apply=%region_2.0 | all-reduce | flops 2 | bytes 16 | tf_op jit(solution)/shard_map/psum | solution.py:73
  159.2 3.1 %subtract_convert_fusion.1 = (bf16[576,576]{1,0:T(8,128)(2,1)S(1)}, f32[576,576]{1,0:T(8,128)}) fusion(f32[576,576]{1,0:T(8,128)} %param.18, f32[576,576]{1,0:T(8,128)} %get-tuple-element.45, f32[]{:T(128)S(6)} %rsqrt.6), kind=kLoop, calls=%fused_computation.1 | loop fusion | flops 1327104 | bytes 4644868 | tf_op jit(solution)/shard_map/convert_element_type | solution.py:79
  162.3 1.2 copy.29
  163.5 0.0 all-gather.5.cloned.1.call-update
  163.5 0.0 all-gather.7.cloned.1.call-start
  163.6 1.6 copy.28
  165.9 3.4 %subtract_convert_fusion = (bf16[576,576]{1,0:T(8,128)(2,1)}, f32[576,576]{1,0:T(8,128)}) fusion(f32[576,576]{1,0:T(8,128)} %param.19, f32[576,576]{0,1:T(8,128)} %copy.28, f32[]{:T(128)S(6)} %rsqrt.7), kind=kLoop, calls=%fused_computation | loop fusion | flops 1327104 | bytes 4644868 | tf_op jit(solution)/shard_map/convert_element_type | solution.py:80
  169.2 0.0 all-gather.7.cloned.1.call-update
  169.3 54.7 %all-gather.5.cloned.1.call-done = bf16[576,2304]{0,1:T(8,128)(2,1)} async-done(((bf16[576,576]{0,1:T(8,128)(2,1)}), bf16[576,2304]{0,1:T(8,128)(2,1)}) %all-gather.5.cloned.1.call-update) | async-done | bytes 2654224 | tf_op jit(solution)/shard_map/all_gather | solution.py:82
  223.9 4.5 %copy.30 = bf16[576,2304]{1,0:T(8,128)(2,1)} copy(bf16[576,2304]{0,1:T(8,128)(2,1)} %all-gather.5.cloned.1.call-done) | data formatting | bytes 5308416
  228.4 56.4 %all-gather.7.cloned.1.call-done = bf16[2304,576]{1,0:T(8,128)(2,1)} async-done(((bf16[576,576]{1,0:T(8,128)(2,1)}), bf16[2304,576]{1,0:T(8,128)(2,1)}) %all-gather.7.cloned.1.call-update) | async-done | bytes 2654224 | tf_op jit(solution)/shard_map/all_gather | solution.py:83
  284.8 4.5 %copy.31 = bf16[2304,576]{0,1:T(8,128)(2,1)} copy(bf16[2304,576]{1,0:T(8,128)(2,1)} %all-gather.7.cloned.1.call-done) | data formatting | bytes 5308416
Async XLA Ops:
  7.2 29.4 %copy-start = (bf16[1024,576]{0,1:T(8,128)(2,1)S(1)}, bf16[1024,576]{0,1:T(8,128)(2,1)}, u32[]{:S(2)}) copy-start(bf16[1024,576]{0,1:T(8,128)(2,1)} %param.15) | copy-start | bytes 3538948
  7.2 67.8 %reduce-scatter.5.cloned.1.call-start = ((), (), s32[]{:S(2)}) async-start(), calls=%async_computation.3 | async-start | bytes 614400 | tf_op jit(solution)/shard_map/reduce_scatter | solution.py:63
  37.2 1.5 copy-start.2
  38.6 59.3 %reduce-scatter.3.cloned.1.call-start = ((), (), s32[]{:S(2)}) async-start(), calls=%async_computation.2 | async-start | bytes 614400 | tf_op jit(solution)/shard_map/reduce_scatter | solution.py:62
  68.7 4.1 %copy-start.1 = (bf16[1024,576]{0,1:T(8,128)(2,1)S(1)}, bf16[1024,576]{0,1:T(8,128)(2,1)}, u32[]{:S(2)}) copy-start(bf16[1024,576]{0,1:T(8,128)(2,1)} %param.14) | copy-start | bytes 3538948
  73.4 1.5 copy-start.4
  73.4 1.5 copy-start.5
  74.8 23.1 %copy-start.6 = (f32[576,48]{0,1:T(8,128)S(1)}, f32[576,48]{0,1:T(8,128)}, u32[]{:S(2)}) copy-start(f32[576,48]{0,1:T(8,128)} %param.21) | copy-start | bytes 331780
  74.8 23.1 %copy-start.7 = (f32[576,48]{0,1:T(8,128)S(1)}, f32[576,48]{0,1:T(8,128)}, u32[]{:S(2)}) copy-start(f32[576,48]{0,1:T(8,128)} %param.20) | copy-start | bytes 331780
  74.9 149.1 %all-gather.5.cloned.1.call-start = ((), (), s32[]{:S(2)}) async-start(), calls=%async_computation.4 | async-start | bytes 3686400 | tf_op jit(solution)/shard_map/all_gather | solution.py:82
  99.6 18.8 %copy-start.3 = (bf16[576,192]{0,1:T(8,128)(2,1)S(1)}, bf16[576,192]{0,1:T(8,128)(2,1)}, u32[]{:S(2)}) copy-start(bf16[576,192]{0,1:T(8,128)(2,1)} %param.17) | copy-start | bytes 663556
  163.5 121.3 %all-gather.7.cloned.1.call-start = ((), (), s32[]{:S(2)}) async-start(), calls=%async_computation.5 | async-start | bytes 3686400 | tf_op jit(solution)/shard_map/all_gather | solution.py:83
Sparse Core Ops, SparseCore 0:
  38.7 25.6 reduce-scatter.4
  75.0 22.8 reduce-scatter.2
  163.6 60.2 all-gather.4
  225.9 58.8 all-gather.6
where the time goes:
time: 296 us
  blocking collectives  125 us (42%)
  waiting for transfers between devices  115 us (39%)
  matrix products  16.5 us (6%)
  between operations  15.3 us (5%)
  local copies, waits for them, and re-layouts  14.7 us (5%)
  other arithmetic  9.81 us (3%)
    all_gather x1, waiting for transfers between devices, per_device(): lax.all_gather(fresh_z, 'fs', axis=0, tiled=True)  56.4 us
    all_gather x1, waiting for transfers between devices, per_device(): lax.all_gather(fresh_out, 'fs', axis=1, tiled=True)  54.7 us
    psum x1, blocking collectives, per_device(): lax.psum((jnp.sum(update_out * update_out), jnp.sum(update_z * update_z))...  38.5 us
    all_gather x1, blocking collectives, per_device(): lax.all_gather(factor_out, 'fs', axis=0, tiled=True)  28.6 us
    all_gather x1, blocking collectives, per_device(): lax.all_gather(factor_z, 'fs', axis=0, tiled=True)  23.8 us
    all_gather x1, blocking collectives, per_device(): lax.all_gather(part_z, 'fs', axis=0, tiled=True)  17.9 us
    all_gather x1, blocking collectives, per_device(): lax.all_gather(part_out, 'fs', axis=1, tiled=True)  16.1 us
    unnamed x20, local copies, waits for them, and re-layouts  10.4 us
  transfers between devices with their start and end apart: 4, of which 3 were waited for; matrix products, arithmetic and copies ran while one was open for 6% of the time, Pallas kernels for 0%

commit v1 on v0

v1 whole, which is shorter than its diff:
```python
import functools

import jax
import jax.numpy as jnp
from jax import lax
from jax.experimental import pallas as pl
from jax.experimental.pallas import tpu as pltpu
from jax.sharding import PartitionSpec as P

beta_first = 0.8
beta_second = 0.9
adam_eps = 1e-08
norm_eps = 1e-06
rate = 0.005

MESH = pl.DeviceIdType.MESH
VMEM = pl.BlockSpec(memory_space=pltpu.VMEM)
PARTS = 4


def remote(src, dst, send, recv, **where):
    return pltpu.make_async_remote_copy(
        src_ref=src, dst_ref=dst, send_sem=send, recv_sem=recv, device_id=where, device_id_type=MESH
    )


def gather_kernel(fs, factor, full, send_z, recv_z, send_x, recv_x, send_c, recv_c, send_d, recv_d):
    me, mine = lax.axis_index("fs"), lax.axis_index("tp")
    part = lax.rem(mine, PARTS)
    far = mine + 2 - 4 * lax.rem(mine // 2, 2)
    near = mine + 1 - 2 * lax.rem(mine, 2)
    far_part = lax.rem(far, PARTS)
    barrier = pltpu.get_barrier_semaphore()
    for d in range(1, fs):
        pl.semaphore_signal(barrier, inc=1, device_id={"fs": lax.rem(me + d, fs)}, device_id_type=MESH)
    for other in (far, near):
        pl.semaphore_signal(barrier, inc=1, device_id={"tp": other}, device_id_type=MESH)
    pl.semaphore_wait(barrier, fs + 1)

    first, second, third, fourth = [], [], [], []
    for d in range(1, fs):
        copy = remote(
            factor.at[part], full.at[me, part], send_z.at[d - 1], recv_z.at[d - 1], fs=lax.rem(me + d, fs)
        )
        copy.start()
        first.append(copy)
    full[me] = factor[...]
    for d in range(1, fs):
        src = lax.rem(me - d + fs, fs)
        first[d - 1].wait_recv()
        block = full.at[src, part]
        copy = remote(block, block, send_x.at[d - 1], recv_x.at[d - 1], tp=far)
        copy.start()
        second.append(copy)
        copy = remote(block, block, send_c.at[d - 1], recv_c.at[d - 1], tp=near)
        copy.start()
        third.append(copy)
    for d in range(1, fs):
        src = lax.rem(me - d + fs, fs)
        second[d - 1].wait_recv()
        block = full.at[src, far_part]
        copy = remote(block, block, send_d.at[d - 1], recv_d.at[d - 1], tp=near)
        copy.start()
        fourth.append(copy)
    for copy in third + fourth:
        copy.wait_recv()
    for copy in first + second + third + fourth:
        copy.wait_send()


def gather_factors(fs, factors):
    parts, rows, columns = factors.shape
    dma = pltpu.SemaphoreType.DMA((fs - 1,))
    return pl.pallas_call(
        functools.partial(gather_kernel, fs),
        out_shape=jax.ShapeDtypeStruct((fs, parts, rows, columns), factors.dtype),
        in_specs=[VMEM],
        out_specs=VMEM,
        scratch_shapes=[dma] * 8,
        compiler_params=pltpu.CompilerParams(collective_id=0, has_side_effects=True),
        cost_estimate=pl.CostEstimate(flops=0, bytes_accessed=30_000_000, transcendentals=0),
    )(factors)


def reduce_kernel(
    fs, tp, term_out, term_z, first, second, full_out, full_z,
    new_first, new_second, dirs, high, low, total,
    arrived, partial, received, send_r, recv_r, send_g, recv_g, send_t, recv_t,
):
    me, mine = lax.axis_index("fs"), lax.axis_index("tp")
    terms = (term_out, term_z)
    fulls = (full_out, full_z)
    rank = first.shape[1]
    barrier = pltpu.get_barrier_semaphore()
    for d in range(1, fs):
        pl.semaphore_signal(barrier, inc=1, device_id={"fs": lax.rem(me + d, fs)}, device_id_type=MESH)
    for d in range(1, tp):
        pl.semaphore_signal(barrier, inc=1, device_id={"tp": lax.rem(mine + d, tp)}, device_id_type=MESH)
    pl.semaphore_wait(barrier, fs + tp - 2)

    sums = []
    for m in range(2):
        for d in range(1, fs):
            peer = lax.rem(me + d, fs)
            copy = remote(
                terms[m].at[peer], arrived.at[m, d - 1], send_r.at[m, d - 1], recv_r.at[m, d - 1], fs=peer
            )
            copy.start()
            sums.append(copy)
    gathers = []
    for m in range(2):
        gradient = terms[m][me]
        for d in range(1, fs):
            sums[m * (fs - 1) + d - 1].wait_recv()
            gradient = gradient + arrived[m, d - 1]
        moment = beta_first * first[m] + (1.0 - beta_first) * gradient
        square = beta_second * second[m] + (1.0 - beta_second) * gradient * gradient
        new_first[m] = moment
        new_second[m] = square
        dirs[m, me] = moment / (jnp.sqrt(square) + adam_eps)
        for d in range(1, fs):
            block = dirs.at[m, me]
            copy = remote(
                block, block, send_g.at[m, d - 1], recv_g.at[m, d - 1], fs=lax.rem(me + d, fs)
            )
            copy.start()
            gathers.append(copy)
    squares = []
    for m in range(2):
        for d in range(1, fs):
            gathers[m * (fs - 1) + d - 1].wait_recv()
        whole = jnp.concatenate([dirs[m, s] for s in range(fs)], axis=0)
        high_part = whole.astype(jnp.bfloat16)
        low_part = (whole - high_part.astype(jnp.float32)).astype(jnp.bfloat16)
        high[m] = high_part
        low[m] = low_part

        def body(s, acc):
            rows = fulls[m][s]
            update = jnp.dot(rows, high[m], preferred_element_type=jnp.float32)
            update = update + jnp.dot(rows, low[m], preferred_element_type=jnp.float32)
            return acc + jnp.sum(update * update, axis=0, keepdims=True)

        acc = lax.fori_loop(0, fs, body, jnp.zeros((1, whole.shape[1]), jnp.float32))
        squares.append(jnp.sum(acc))
    row = lax.broadcasted_iota(jnp.int32, partial.shape, 0)
    partial[...] = jnp.where(row == 0, squares[0], squares[1])
    totals = []
    for d in range(1, tp):
        copy = remote(
            partial, received.at[d - 1], send_t.at[d - 1], recv_t.at[d - 1], tp=lax.rem(mine + d, tp)
        )
        copy.start()
        totals.append(copy)
    result = partial[...]
    for d in range(1, tp):
        totals[d - 1].wait_recv()
        result = result + received[d - 1]
    total[...] = result
    for copy in sums + gathers + totals:
        copy.wait_send()


def reduce_moments(fs, tp, term_out, term_z, first, second, full_out, full_z):
    _, rank, inner = first.shape
    dma = pltpu.SemaphoreType.DMA
    shape = jax.ShapeDtypeStruct
    f32, bf16 = jnp.float32, jnp.bfloat16
    return pl.pallas_call(
        functools.partial(reduce_kernel, fs, tp),
        out_shape=(
            shape(first.shape, f32),
            shape(first.shape, f32),
            shape((2, fs, rank, inner), f32),
            shape((2, fs * rank, inner), bf16),
            shape((2, fs * rank, inner), bf16),
            shape((8, 128), f32),
        ),
        in_specs=[VMEM] * 6,
        out_specs=[VMEM] * 6,
        scratch_shapes=[
            pltpu.VMEM((2, fs - 1, rank, inner), f32),
            pltpu.VMEM((8, 128), f32),
            pltpu.VMEM((tp - 1, 8, 128), f32),
            dma((2, fs - 1)),
            dma((2, fs - 1)),
            dma((2, fs - 1)),
            dma((2, fs - 1)),
            dma((tp - 1,)),
            dma((tp - 1,)),
        ],
        compiler_params=pltpu.CompilerParams(
            collective_id=1, has_side_effects=True, vmem_limit_bytes=48 * 1024 * 1024
        ),
        cost_estimate=pl.CostEstimate(flops=0, bytes_accessed=100_000_000, transcendentals=0),
    )(term_out, term_z, first, second, full_out, full_z)


def copies_kernel(fs, own_out, own_z, all_out, all_z, kept, send_a, recv_a, send_b, recv_b):
    me = lax.axis_index("fs")
    barrier = pltpu.get_barrier_semaphore()

    @pl.when(me > 0)
    def _():
        pl.semaphore_signal(barrier, inc=1, device_id={"fs": me - 1}, device_id_type=MESH)

    @pl.when(me < fs - 1)
    def _():
        pl.semaphore_signal(barrier, inc=1, device_id={"fs": me + 1}, device_id_type=MESH)

    pl.semaphore_wait(barrier, jnp.minimum(me, 1) + jnp.minimum(fs - 1 - me, 1))

    owns, alls = (own_out, own_z), (all_out, all_z)
    local = [pltpu.make_async_copy(owns[m], alls[m].at[me], kept.at[m]) for m in range(2)]
    for copy in local:
        copy.start()

    def up(m, src, block, step):
        return remote(block, alls[m].at[src], send_a.at[m, step], recv_a.at[m, step], fs=me + 1)

    def down(m, src, block, step):
        return remote(block, alls[m].at[src], send_b.at[m, step], recv_b.at[m, step], fs=me - 1)

    for step in range(fs - 1):
        for m in range(2):
            below, above = me - step, me + step
            held_below = jnp.maximum(below, 0)
            held_above = jnp.minimum(above, fs - 1)
            if step > 0:
                @pl.when(below >= 0)
                def _(m=m, held_below=held_below, step=step):
                    block = alls[m].at[held_below]
                    up(m, held_below, block, step - 1).wait_recv()

                @pl.when(above < fs)
                def _(m=m, held_above=held_above, step=step):
                    block = alls[m].at[held_above]
                    down(m, held_above, block, step - 1).wait_recv()

            @pl.when((below >= 0) & (me < fs - 1))
            def _(m=m, held_below=held_below, step=step):
                block = owns[m] if step == 0 else alls[m].at[held_below]
                up(m, held_below, block, step).start()

            @pl.when((above < fs) & (me > 0))
            def _(m=m, held_above=held_above, step=step):
                block = owns[m] if step == 0 else alls[m].at[held_above]
                down(m, held_above, block, step).start()

    last = fs - 2
    for m in range(2):
        @pl.when(me - last - 1 >= 0)
        def _(m=m):
            up(m, 0, alls[m].at[0], last).wait_recv()

        @pl.when(me + last + 1 < fs)
        def _(m=m):
            down(m, 0, alls[m].at[0], last).wait_recv()

    for step in range(fs - 1):
        for m in range(2):
            @pl.when((me - step >= 0) & (me < fs - 1))
            def _(m=m, step=step):
                up(m, 0, owns[m], step).wait_send()

            @pl.when((me + step < fs) & (me > 0))
            def _(m=m, step=step):
                down(m, 0, owns[m], step).wait_send()
    for copy in local:
        copy.wait()


def gather_copies(fs, own_out, own_z):
    dma = pltpu.SemaphoreType.DMA((2, fs - 1))
    return pl.pallas_call(
        functools.partial(copies_kernel, fs),
        out_shape=tuple(jax.ShapeDtypeStruct((fs,) + own.shape, own.dtype) for own in (own_out, own_z)),
        in_specs=[VMEM] * 2,
        out_specs=[VMEM] * 2,
        scratch_shapes=[pltpu.SemaphoreType.DMA((2,)), dma, dma, dma, dma],
        compiler_params=pltpu.CompilerParams(collective_id=2, has_side_effects=True),
        cost_estimate=pl.CostEstimate(flops=0, bytes_accessed=100_000_000, transcendentals=0),
    )(own_out, own_z)


def split_parts(values):
    high_part = values.astype(jnp.bfloat16)
    low_part = (values - high_part.astype(jnp.float32)).astype(jnp.bfloat16)
    return (high_part, low_part)


def per_device(
    fs, tp,
    block_in, out_cot, gated_out, gate_cot, factor_out, factor_z,
    weight_out, weight_z, first_out, second_out, first_z, second_z,
):
    width, rank = factor_out.shape[0], factor_out.shape[1]
    inner = gated_out.shape[1]
    entries = width * fs * inner * tp

    both = jnp.concatenate([factor_out, factor_z], axis=1).reshape(PARTS, width // PARTS, 2 * rank)
    full = gather_factors(fs, both).reshape(width * fs, 2 * rank)
    full_out, full_z = full[:, :rank], full[:, rank:]

    def term(values, factor, other):
        proj = jnp.dot(values, factor, preferred_element_type=jnp.float32)
        high_part, low_part = split_parts(proj)
        return jnp.dot(high_part.T, other, preferred_element_type=jnp.float32) + jnp.dot(
            low_part.T, other, preferred_element_type=jnp.float32
        )

    term_out = term(out_cot, full_out, gated_out).reshape(fs, rank // fs, inner)
    term_z = term(block_in, full_z, gate_cot).reshape(fs, rank // fs, inner)
    new_first, new_second, _, high, low, total = reduce_moments(
        fs, tp, term_out, term_z,
        jnp.stack([first_out.T, first_z]), jnp.stack([second_out.T, second_z]),
        full_out.reshape(fs, width, rank), full_z.reshape(fs, width, rank),
    )
    scale_out = lax.rsqrt(total[0, 0] / entries + norm_eps)
    scale_z = lax.rsqrt(total[1, 0] / entries + norm_eps)
    pair = jnp.concatenate([high, low], axis=1)

    def twice(factor):
        return jnp.concatenate([factor, factor], axis=1)

    def of_out(factor):
        return lax.dot_general(
            pair[0], twice(factor), (((0,), (1,)), ((), ())), preferred_element_type=jnp.float32
        )

    def of_z(factor):
        return jnp.dot(twice(factor), pair[1], preferred_element_type=jnp.float32)

    step_out = of_out(factor_out) * scale_out
    step_z = of_z(factor_z) * scale_z
    fresh_out = (weight_out - rate * step_out).astype(jnp.bfloat16)
    fresh_z = (weight_z - rate * step_z).astype(jnp.bfloat16)
    copies_out, copies_z = gather_copies(fs, fresh_out, fresh_z)
    copy_out = copies_out.transpose(1, 0, 2).reshape(inner, fs * width)
    copy_z = copies_z.reshape(fs * width, inner)
    return (
        step_out, step_z,
        new_first[0].T, new_second[0].T, new_first[1], new_second[1],
        copy_out, copy_z,
    )


def solution(mesh):
    return jax.shard_map(
        functools.partial(per_device, mesh.shape["fs"], mesh.shape["tp"]),
        mesh=mesh,
        in_specs=(
            P("fs", None),
            P("fs", None),
            P("fs", "tp"),
            P("fs", "tp"),
            P("fs", None),
            P("fs", None),
            P("tp", "fs"),
            P("fs", "tp"),
            P("tp", "fs"),
            P("tp", "fs"),
            P("fs", "tp"),
            P("fs", "tp"),
        ),
        out_specs=(
            P("tp", "fs"),
            P("fs", "tp"),
            P("tp", "fs"),
            P("tp", "fs"),
            P("fs", "tp"),
            P("fs", "tp"),
            P("tp", None),
            P(None, "tp"),
        ),
        check_vma=False,
    )
```

time: 296 us -> 221 us (0.75)
  Pallas kernels: 0 us -> 181 us
  blocking collectives: 125 us -> 0 us
  waiting for transfers between devices: 115 us -> 0 us
  between operations: 15.3 us -> 2.16 us
  other arithmetic: 9.81 us -> 3.17 us
  local copies, waits for them, and re-layouts: 14.7 us -> 19.1 us
    pallas_call x0 -> x3, Pallas kernels: none -> 181 us  [the longest x1 103 us: gather_copies(): pl.pallas_call(functools.partial(copies_kernel, fs), out_shape=tuple((jax...]
    all_gather x2 -> x0, waiting for transfers between devices: 111 us -> none  [the longest x1 56.4 us: per_device(): lax.all_gather(fresh_z, 'fs', axis=0, tiled=True)]
    all_gather x4 -> x0, blocking collectives: 86.4 us -> none  [the longest x1 28.6 us: per_device(): lax.all_gather(factor_out, 'fs', axis=0, tiled=True)]
    psum x1 -> x0, blocking collectives: 38.5 us -> none  [per_device(): lax.psum((jnp.sum(update_out * update_out), jnp.sum(update_z * update_z))...]
    convert_element_type x2 -> x0, other arithmetic: 6.5 us -> none  [the longest x1 3.37 us: per_device(): fresh_z = (weight_z - rate * step_z).astype(jnp.bfloat16)]
    transpose x0 -> x1, local copies, waits for them, and re-layouts: none -> 4.68 us  [per_device(): copy_out = copies_out.transpose(1, 0, 2).reshape(inner, fs * width)]
    reduce_scatter x2 -> x0, waiting for transfers between devices: 3.37 us -> none  [the longest x1 3.35 us: per_device(): lax.psum_scatter(term_out, 'fs', scatter_dimension=1, tiled=True)]
    div x2 -> x0, other arithmetic: 3.31 us -> none  [moments(): new_first / (jnp.sqrt(new_second) + adam_eps)]
  transfers between devices with their start and end apart: 4 -> 0, of which waited for: 3 -> 0; matrix products, arithmetic and copies ran while one was open for 6% -> 0% of each run, Pallas kernels for 0% -> 0%
where the time goes in v1:
time: 221 us; the launch traced here: 220 us
  Pallas kernels  181 us (82%)
  local copies, waits for them, and re-layouts  19.1 us (9%)
  matrix products  15.4 us (7%)
  other arithmetic  3.17 us (1%)
    pallas_call x1, Pallas kernels, gather_copies(): pl.pallas_call(functools.partial(copies_kernel, fs), out_shape=tuple((jax...  103 us
    pallas_call x1, Pallas kernels, reduce_moments(): pl.pallas_call(functools.partial(reduce_kernel, fs, tp), out_shape=(shape...  54.1 us
    pallas_call x1, Pallas kernels, gather_factors(): pl.pallas_call(functools.partial(gather_kernel, fs), out_shape=jax.ShapeD...  23.3 us
    unnamed x17, local copies, waits for them, and re-layouts  10.5 us
    dot_general x2, matrix products, term(): proj = jnp.dot(values, factor, preferred_element_type=jnp.float32)  8.99 us
    transpose x1, local copies, waits for them, and re-layouts, per_device(): copy_out = copies_out.transpose(1, 0, 2).reshape(inner, fs * width)  4.68 us

profile of v1, /device:TPU:0, one launch (start us, length us, event | category | flops | bytes accessed | tf_op | source)
XLA Modules:
  0.0 220.3 jit_solution(9607941696244868244)
XLA Ops:
  0.6 0.0 copy-start
  0.6 1.1 pad_maximum_fusion.5.first
  1.7 1.0 pad_maximum_fusion.6.second
  2.7 1.1 pad_maximum_fusion.1
  3.8 1.0 copy.22
  4.8 23.3 %shard_map.179 = bf16[4,4,144,384]{3,2,1,0:T(8,128)(2,1)} custom-call(bf16[4,144,384]{2,1,0:T(8,128)(2,1)} %bitcast.61), custom_call_target="tpu_custom_call" | custom-call | bytes 30000000 | tf_op jit(solution)/shard_map/pallas_call | solution.py:74
  28.1 4.8 %convolution_bitcast_fusion = f32[1024,192]{0,1:T(8,128)S(1)} fusion(bf16[1024,2304]{1,0:T(8,128)(2,1)} %param.12, bf16[2304,384]{1,0:T(8,128)(2,1)} %bitcast.55), kind=kOutput, calls=%fused_computation.4 | convolution fusion | flops 905969664 | bytes 6684672 | tf_op jit(solution)/shard_map/dot_general | solution.py:306
  32.9 0.0 copy-done
  32.9 0.6 fusion.3
  33.5 0.0 copy-start.1
  33.6 0.6 convolution_add_fusion
  34.2 0.9 copy-done.1
  35.0 0.0 copy-start.2
  35.0 4.2 %convolution_bitcast_fusion.1 = f32[1024,192]{0,1:T(8,128)S(1)} fusion(bf16[1024,2304]{1,0:T(8,128)(2,1)} %param.13, bf16[2304,384]{1,0:T(8,128)(2,1)S(1)} %bitcast.56), kind=kOutput, calls=%fused_computation.5 | convolution fusion | flops 905969664 | bytes 6684672 | tf_op jit(solution)/shard_map/dot_general | solution.py:306
  39.2 0.0 copy-done.2
  39.2 0.6 fusion.6
  39.8 0.6 convolution_add_fusion.1
  40.4 1.5 fusion.12
  41.9 54.1 %shard_map.180 = (f32[2,48,576]{2,1,0:T(8,128)S(1)}, f32[2,48,576]{2,1,0:T(8,128)S(1)}, f32[2,4,48,576]{3,2,1,0:T(8,128)}, bf16[2,192,576]{2,1,0:T(8,128)(2,1)S(...) custom-call(f32[4,48,576]{2,1,0:T(8,128)S(1)} %bitcast.53, f32[4,48,576]{2,1,0:T(8,128)S(1)} %bitcast.52, ...), custom_call_target="tpu_custom_call" | custom-call | bytes 100000000 | tf_op jit(solution)/shard_map/pallas_call | solution.py:169
  96.1 0.5 fusion.13
  98.0 0.0 copy-start.3
  98.0 0.0 copy-start.5
  98.0 0.1 constant_dynamic-update-slice_fusion
  98.1 0.8 slice_bitcast_fusion.4
  98.9 0.6 copy-done.3
  99.5 0.0 copy-done.5
  99.5 0.0 copy-start.4
  99.5 0.0 copy-start.6
  99.5 2.0 subtract_convert_fusion
  101.5 0.0 copy-done.4
  101.5 0.0 copy-done.6
  101.5 2.0 subtract_convert_fusion.1
  103.5 103.1 %shard_map.181 = (bf16[4,576,576]{2,1,0:T(8,128)(2,1)}, bf16[4,576,576]{2,1,0:T(8,128)(2,1)}) custom-call(bf16[576,576]{1,0:T(8,128)(2,1)} %get-tuple-element.46.own_out, bf16[576,576]{1,0:T(8,128)(2,1)} %get-tuple-element.48.own_z), custom_call_target="tpu_custom_call" | custom-call | bytes 100000000 | tf_op jit(solution)/shard_map/pallas_call | solution.py:275
  206.6 4.7 %copy.23 = bf16[576,4,576]{0,2,1:T(8,128)(2,1)} copy(bf16[576,4,576]{2,0,1:T(8,128)(2,1)} %bitcast.60) | data formatting | bytes 5308416 | tf_op jit(solution)/shard_map/transpose | solution.py:339
  211.3 4.5 %copy.24 = bf16[576,2304]{1,0:T(8,128)(2,1)} copy(bf16[576,2304]{0,1:T(8,128)(2,1)} %bitcast.54) | data formatting | bytes 5308416
  215.8 4.5 %copy.25 = bf16[2304,576]{0,1:T(8,128)(2,1)} copy(bf16[2304,576]{1,0:T(8,128)(2,1)} %bitcast.59) | data formatting | bytes 5308416
  (1 shorter events, 0.0 us)
Async XLA Ops:
  0.6 32.3 %copy-start = (bf16[1024,576]{0,1:T(8,128)(2,1)S(1)}, bf16[1024,576]{0,1:T(8,128)(2,1)}, u32[]{:S(2)}) copy-start(bf16[1024,576]{0,1:T(8,128)(2,1)} %param.15) | copy-start | bytes 3538948
  33.5 1.5 copy-start.1
  35.0 4.2 %copy-start.2 = (bf16[1024,576]{0,1:T(8,128)(2,1)S(1)}, bf16[1024,576]{0,1:T(8,128)(2,1)}, u32[]{:S(2)}) copy-start(bf16[1024,576]{0,1:T(8,128)(2,1)} %param.14) | copy-start | bytes 3538948
  98.0 1.6 copy-start.3
  98.0 1.6 copy-start.5
  99.5 2.0 copy-start.4
  99.5 2.0 copy-start.6
